TPU v7x, 32 devices: a whole 2x2x4 slice. The times are simulated.
32 devices in a mesh: sp: 8 (over z, y), tp: 4 (over x, core).
Axes of the slice: x: 2, y: 2, z: 4, core: 2. Of those that a mesh axis runs over, the one named last changes fastest.
Arguments:
- queries: bfloat16 [2048, 2048], P('sp', 'tp'), may hold values from -6 to 6
- keys: bfloat16 [2048, 512], P('sp', 'tp'), may hold values from -6 to 6
- values: bfloat16 [2048, 512], P('sp', 'tp'), may hold values from -6 to 6
- query_gain: float32 [64], replicated, may hold values from 0.8 to 5
- key_gain: float32 [64], replicated, may hold values from 0.8 to 5
- stream: bfloat16 [2048, 2048], P('sp'), may hold values from -0.1796875 to 0.1796875
- out_weight: bfloat16 [2048, 2048], P('tp'), may hold values from -0.125 to 0.125
- mixer_gain: float32 [2048], replicated, may hold values from 0.1 to 1.9
- up_weight: bfloat16 [2048, 8192], P('sp', 'tp'), may hold values from -0.125 to 0.125
- down_weight: bfloat16 [8192, 2048], P('tp', 'sp'), may hold values from -0.0625 to 0.0625
Outputs:
- updated: bfloat16 [2048, 2048], P('sp', 'tp')
All inputs are finite; a program needn't handle non-finite values.
Results may differ from a plain program's by a relative error of at most 0.02.
The roundings to bfloat16 on the way count: a program that leaves them out, or rounds other values in their place, can miss the bound.
Values may be sent and summed in bfloat16 or wider, within the bound.
A program may use at most 128 MiB of HBM per device.

v0:
```python
import math
import jax
import jax.numpy as jnp
from jax import lax
from jax.sharding import PartitionSpec as P

HD = 64
GRID_W = 64
EPSILON = 1e-06


def prepare(projected, gain_vec, offset):
    row_count = projected.shape[0]
    head_count = projected.shape[1] // HD
    widened = projected.astype(jnp.float32).reshape(row_count, head_count, HD)
    widened = (
        widened
        * lax.rsqrt(jnp.mean(widened * widened, axis=-1, keepdims=True) + EPSILON)
        * gain_vec
    )
    position = offset + jnp.arange(row_count, dtype=jnp.int32)
    grid_row = (position // GRID_W).astype(jnp.float32)
    grid_col = (position % GRID_W).astype(jnp.float32)
    half_dim = HD // 2
    inverse = 1.0 / jnp.power(10000.0, jnp.arange(0, half_dim, 2, dtype=jnp.float32) / half_dim)
    angle = jnp.concatenate([grid_row[:, None] * inverse, grid_col[:, None] * inverse], axis=-1)
    cosine = jnp.cos(angle)[:, None, :]
    sine_table = jnp.sin(angle)[:, None, :]
    paired = widened.reshape(row_count, head_count, half_dim, 2)
    former = paired[..., 0]
    latter = paired[..., 1]
    rotated = jnp.stack(
        [former * cosine - latter * sine_table, former * sine_table + latter * cosine], axis=-1
    )
    return rotated.reshape(row_count, head_count, HD).astype(jnp.bfloat16)


def attend_block(state, grouped, key_block, value_block):
    running, totals, weighted = state
    scores = jnp.einsum("qhgd,khd->hgqk", grouped, key_block, preferred_element_type=jnp.float32)
    scores = scores * (1.0 / math.sqrt(HD))
    newest = jnp.maximum(running, jnp.max(scores, axis=-1))
    rescale = jnp.exp(running - newest)
    exps = jnp.exp(scores - newest[..., None])
    totals = totals * rescale + jnp.sum(exps, axis=-1)
    weighted = weighted * rescale[..., None] + jnp.einsum(
        "hgqk,khd->hgqd", exps.astype(jnp.bfloat16), value_block, preferred_element_type=jnp.float32
    )
    return (newest, totals, weighted)


def shards(
    queries,
    keys,
    values,
    query_gain,
    key_gain,
    stream,
    out_weight,
    mixer_gain,
    up_weight,
    down_weight,
):
    local_rows = queries.shape[0]
    offset = lax.axis_index("sp") * local_rows
    kv_count = keys.shape[1] // HD
    group_size = queries.shape[1] // HD // kv_count
    grouped = prepare(queries, query_gain, offset).reshape(local_rows, kv_count, group_size, HD)
    prepared_keys = prepare(keys, key_gain, offset).reshape(local_rows, kv_count * HD)
    initial = (
        jnp.full((kv_count, group_size, local_rows), -1e30, jnp.float32),
        jnp.zeros((kv_count, group_size, local_rows), jnp.float32),
        jnp.zeros((kv_count, group_size, local_rows, HD), jnp.float32),
    )
    key_rows = lax.all_gather(prepared_keys, "sp", axis=0, tiled=True)
    value_rows = lax.all_gather(values, "sp", axis=0, tiled=True)
    piece_rows = key_rows.shape[0]
    block_rows = piece_rows if piece_rows <= 2048 else math.gcd(piece_rows, 2048)
    key_blocks = key_rows.reshape(piece_rows // block_rows, block_rows, kv_count, HD)
    value_blocks = value_rows.reshape(piece_rows // block_rows, block_rows, kv_count, HD)

    def visit_block(block_index, state_now):
        return attend_block(state_now, grouped, key_blocks[block_index], value_blocks[block_index])

    running, totals, weighted = lax.fori_loop(0, piece_rows // block_rows, visit_block, initial)
    head_out = weighted / totals[..., None]
    head_out = jnp.transpose(head_out, (2, 0, 1, 3)).reshape(local_rows, -1).astype(jnp.bfloat16)
    partial_value = jnp.dot(head_out, out_weight, preferred_element_type=jnp.float32)
    model_width = partial_value.shape[1]
    share_cols = model_width // lax.axis_size("tp")
    first_col = lax.axis_index("tp") * share_cols
    summed = lax.psum(partial_value.astype(jnp.bfloat16), "tp").astype(jnp.float32)
    mid = (stream.astype(jnp.float32) + summed).astype(jnp.bfloat16)
    mid_wide = mid.astype(jnp.float32)
    normed = (
        mid_wide
        * lax.rsqrt(jnp.mean(mid_wide * mid_wide, axis=-1, keepdims=True) + EPSILON)
        * mixer_gain
    )
    normed = normed.astype(jnp.bfloat16)
    own_mid = lax.dynamic_slice_in_dim(mid, first_col, share_cols, 1)
    up_sums = jnp.dot(
        normed,
        lax.all_gather(up_weight, "sp", axis=0, tiled=True),
        preferred_element_type=jnp.float32,
    )
    hidden = jnp.square(jax.nn.relu(up_sums)).astype(jnp.bfloat16)
    down_part = jnp.dot(
        hidden,
        lax.all_gather(down_weight, "sp", axis=1, tiled=True),
        preferred_element_type=jnp.float32,
    )
    down_share = lax.psum_scatter(
        down_part.astype(jnp.bfloat16), "tp", scatter_dimension=1, tiled=True
    ).astype(jnp.float32)
    return (own_mid.astype(jnp.float32) + down_share).astype(jnp.bfloat16)


def solution(mesh):
    return jax.shard_map(
        shards,
        mesh=mesh,
        in_specs=(
            P("sp", "tp"),
            P("sp", "tp"),
            P("sp", "tp"),
            P(),
            P(),
            P("sp", None),
            P("tp", None),
            P(),
            P("sp", "tp"),
            P("tp", "sp"),
        ),
        out_specs=P("sp", "tp"),
        check_vma=False,
    )
```

profile of v0, /device:TPU:0, one launch (start us, length us, event | category | flops | bytes accessed | tf_op | source)
XLA Modules:
  0.0 400.8 jit_solution(354414603991874629)
XLA Ops:
  7.4 0.0 copy-start
  7.4 0.0 all-reduce.2.cloned.1.call-start
  7.4 1.2 copy.18
  8.6 0.3 reshape.165
  8.9 0.1 bitcast_reduce_fusion.1
  9.0 0.9 copy.17
  9.9 0.1 reshape.164
  10.1 0.8 mul.244
  10.8 0.1 broadcast_multiply_fusion.1
  10.9 0.1 fusion.28
  11.0 0.3 multiply_multiply_fusion
  11.3 0.7 subtract_convert_fusion
  12.0 0.6 pad_maximum_fusion
  12.6 0.1 convert_element_type.81
  12.7 0.8 mul.225
  13.5 0.1 multiply_multiply_fusion.1
  13.6 0.2 subtract_convert_fusion.1
  13.8 0.2 pad_maximum_fusion.1
  14.0 33.0 %all_gather.12 = bf16[2048,128]{0,1:T(8,128)(2,1)S(1)} all-gather(bf16[256,128]{0,1:T(8,128)(2,1)S(1)} %convert_element_type.79), channel_id=1, replica_groups=mesh['sp'=8,'tp'=4] {'sp'}, dimensions={0}, use_global_device_ids=true | all-gather | bytes 589824 | tf_op jit(solution)/shard_map/all_gather | solution.py:75
  47.0 8.1 %bitcast_reduce_fusion = (f32[2,4,256]{2,1,0:T(4,128)S(1)}, f32[2,2048,256,4]{2,1,3,0:T(8,128)}) fusion(bf16[2048,2,64,1]{0,2,3,1:T(8,128)(2,1)S(1)} %bitcast.63, bf16[256,2,4,64]{0,3,2,1:T(8,128)(2,1)S(1)} %convert_element_type.81), kind=kOutput, calls=%fused_computation.1 | convolution fusion | flops 545257472 | bytes 17571840 | tf_op jit(solution)/shard_map/while/body/eval_jaxpr/qhgd,khd->hgqk/dot_general | solution.py:40
  55.1 0.0 copy-start.1
  55.1 8.5 %fusion.1 = f32[2,4,256]{2,1,0:T(4,128)S(1)} fusion(f32[2,2048,256,4]{2,1,3,0:T(8,128)} %get-tuple-element.42, f32[2,4,256]{2,1,0:T(4,128)S(1)} %get-tuple-element.38), kind=kLoop, calls=%fused_computation.3 | loop fusion | flops 12580864 | bytes 16793600 | tf_op jit(solution)/shard_map/while/body/eval_jaxpr/reduce_sum | solution.py:45
  63.7 0.0 copy-done.1
  63.7 31.3 %all_gather.13 = bf16[2048,128]{1,0:T(8,128)(2,1)S(1)} all-gather(bf16[256,128]{1,0:T(8,128)(2,1)S(1)} %copy-done.1), channel_id=1, replica_groups=mesh['sp'=8,'tp'=4] {'sp'}, dimensions={0}, use_global_device_ids=true | all-gather | bytes 589824 | tf_op jit(solution)/shard_map/all_gather | solution.py:76
  95.0 0.2 copy.19
  95.2 7.4 %fusion.22 = bf16[256,2,4,64]{0,3,2,1:T(8,128)(2,1)S(1)} fusion(bf16[2048,2,64,1]{0,2,3,1:T(8,128)(2,1)S(1)} %bitcast.62, f32[2,2048,256,4]{2,1,3,0:T(8,128)} %get-tuple-element.42, f32[2,4,256]{2,1,0:T(4,128)S(1)} %get-tuple-element.38, f32[256,2,4]{0,2,1:T(4,128)S(1)} %bitcast_add_fusion, f32[256,2,4]{0,2,1:T(4,128)S(1)} %get-tuple-element.37), kind=kOutput, calls=%fused_computation.22 | convolution fusion | flops 549847040 | bytes 17588224 | tf_op jit(solution)/shard_map/while/body/eval_jaxpr/hgqk,khd->hgqd/dot_general | solution.py:46
  102.6 0.0 copy-start.2
  102.6 0.0 copy-done
  102.6 1.8 convolution_convert_fusion
  104.3 0.0 all-reduce.2.cloned.1.call-update
  104.4 0.0 all-gather.3.cloned.1.call-start
  104.4 0.5 all-gather.3.cloned.1.call-update
  104.9 0.0 all-gather.5.cloned.1.call-start
  105.0 0.5 all-gather.5.cloned.1.call-update
  105.5 0.2 reduce-scatter.2.cloned.1.call-start
  105.8 36.5 %all-reduce.2.cloned.1.call-done = bf16[256,2048]{1,0:T(8,128)(2,1)} async-done(((bf16[256,2048]{1,0:T(8,128)(2,1)}), bf16[256,2048]{1,0:T(8,128)(2,1)}) %all-reduce.2.cloned.1.call-update) | async-done | bytes 1048592 | tf_op jit(solution)/shard_map/psum | solution.py:92
  142.3 2.1 fusion.7
  144.4 88.0 %all-gather.3.cloned.1.call-done = bf16[2048,2048]{1,0:T(8,128)(2,1)} async-done(((bf16[256,2048]{1,0:T(8,128)(2,1)}), bf16[2048,2048]{1,0:T(8,128)(2,1)}) %all-gather.3.cloned.1.call-update) | async-done | bytes 8388624 | tf_op jit(solution)/shard_map/all_gather | solution.py:104
  232.4 124.8 %all-gather.5.cloned.1.call-done = bf16[2048,2048]{1,0:T(8,128)(2,1)} async-done(((bf16[2048,256]{1,0:T(8,128)(2,1)}), bf16[2048,2048]{1,0:T(8,128)(2,1)}) %all-gather.5.cloned.1.call-update) | async-done | bytes 8388624 | tf_op jit(solution)/shard_map/all_gather | solution.py:110
  357.2 0.0 copy-done.2
  357.2 11.3 %convolution_convert_fusion.1 = bf16[256,2048]{1,0:T(8,128)(2,1)} fusion(bf16[2048,2048]{1,0:T(8,128)(2,1)} %all-gather.5.cloned.1.call-done, bf16[2048,2048]{1,0:T(8,128)(2,1)} %all-gather.3.cloned.1.call-done, bf16[256,2048]{1,0:T(8,128)(2,1)S(1)} %get-tuple-element.20, f32[2048]{0:T(1024)S(1)} %copy-done.2, f32[256]{0:T(256)S(1)} %add_rsqrt_fusion.2), kind=kOutput, calls=%fused_computation.12 | convolution fusion | flops 4299161600 | bytes 18883584 | tf_op jit(solution)/shard_map/dot_general | solution.py:108
  368.5 0.0 reduce-scatter.2.cloned.1.call-update
  368.5 23.1 %reduce-scatter.2.cloned.1.call-done = bf16[256,512]{1,0:T(8,128)(2,1)} async-done(((bf16[256,2048]{1,0:T(8,128)(2,1)}), bf16[256,512]{1,0:T(8,128)(2,1)}) %reduce-scatter.2.cloned.1.call-update) | async-done | bytes 262160 | tf_op jit(solution)/shard_map/reduce_scatter | solution.py:113
  391.6 1.7 add_convert_fusion.1
  (9 shorter events, 0.1 us)
Async XLA Ops:
  7.4 95.2 %copy-start = (bf16[512,2048]{1,0:T(8,128)(2,1)S(1)}, bf16[512,2048]{1,0:T(8,128)(2,1)}, u32[]{:S(2)}) copy-start(bf16[512,2048]{1,0:T(8,128)(2,1)} %param.16) | copy-start | bytes 6291460
  7.4 134.9 %all-reduce.2.cloned.1.call-start = ((), (), s32[]{:S(2)}) async-start(), calls=%async_computation.1 | async-start | bytes 2097152 | tf_op jit(solution)/shard_map/psum | solution.py:92
  55.1 8.6 %copy-start.1 = (bf16[256,128]{1,0:T(8,128)(2,1)S(1)}, bf16[256,128]{1,0:T(8,128)(2,1)}, u32[]{:S(2)}) copy-start(bf16[256,128]{1,0:T(8,128)(2,1)} %param.12) | copy-start | bytes 196612
  102.6 254.6 %copy-start.2 = (f32[2048]{0:T(1024)S(1)}, f32[2048]{0:T(1024)}, u32[]{:S(2)}) copy-start(f32[2048]{0:T(1024)} %param.17) | copy-start | bytes 24580
  104.4 128.0 %all-gather.3.cloned.1.call-start = ((), (), s32[]{:S(2)}) async-start(), calls=%async_computation.2 | async-start | bytes 9437184 | tf_op jit(solution)/shard_map/all_gather | solution.py:104
  104.9 252.3 %all-gather.5.cloned.1.call-start = ((), (), s32[]{:S(2)}) async-start(), calls=%async_computation.3 | async-start | bytes 9437184 | tf_op jit(solution)/shard_map/all_gather | solution.py:110
  105.5 286.1 %reduce-scatter.2.cloned.1.call-start = ((), (), s32[]{:S(2)}) async-start(), calls=%async_computation.4 | async-start | bytes 1310720 | tf_op jit(solution)/shard_map/reduce_scatter | solution.py:113
Sparse Core Ops, SparseCore 0:
  104.5 37.7 all-reduce.1
  368.6 22.9 reduce-scatter.1
Sparse Core Ops, SparseCore 1:
  107.0 125.3 all-gather.2
  234.3 122.9 all-gather.4
where the time goes:
time: 401 us
  waiting for transfers between devices  274 us (68%)
  blocking collectives  64.3 us (16%)
  matrix products  28.5 us (7%)
  between operations  15.1 us (4%)
  other arithmetic  14.7 us (4%)
  local copies, waits for them, and re-layouts  4.36 us (1%)
    all_gather x1, waiting for transfers between devices, shards(): lax.all_gather(down_weight, 'sp', axis=1, tiled=True)  125 us
    all_gather x1, waiting for transfers between devices, shards(): lax.all_gather(up_weight, 'sp', axis=0, tiled=True)  88 us
    psum x1, waiting for transfers between devices, shards(): lax.psum(partial_value.astype(jnp.bfloat16), 'tp').astype(jnp.float32)  36.5 us
    all_gather x1, blocking collectives, shards(): key_rows = lax.all_gather(prepared_keys, 'sp', axis=0, tiled=True)  33 us
    all_gather x1, blocking collectives, shards(): value_rows = lax.all_gather(values, 'sp', axis=0, tiled=True)  31.3 us
    reduce_scatter x1, waiting for transfers between devices, shards(): lax.psum_scatter(down_part.astype(jnp.bfloat16), 'tp', scatter_dimension=...  23.1 us
    dot_general x1, matrix products, shards(): jnp.dot(hidden, lax.all_gather(down_weight, 'sp', axis=1, tiled=True), pr...  11.3 us
    reduce_sum x1, other arithmetic, attend_block(): totals = totals * rescale + jnp.sum(exps, axis=-1)  8.52 us
  transfers between devices with their start and end apart: 4, of which 4 were waited for; matrix products, arithmetic and copies ran while one was open for 1% of the time, Pallas kernels for 0%

commit v1 on v0

--- a/solution.py
+++ b/solution.py
@@ -7,6 +7,12 @@
 HD = 64
 GRID_W = 64
 EPSILON = 1e-06
+
+
+def gather_and_add(shard, name):
+    terms = lax.all_gather(shard, name, axis=0, tiled=False)
+    result = terms.sum(axis=0)
+    return result
 
 
 def prepare(projected, gain_vec, offset):
@@ -89,7 +95,7 @@
     model_width = partial_value.shape[1]
     share_cols = model_width // lax.axis_size("tp")
     first_col = lax.axis_index("tp") * share_cols
-    summed = lax.psum(partial_value.astype(jnp.bfloat16), "tp").astype(jnp.float32)
+    summed = gather_and_add(partial_value.astype(jnp.bfloat16), "tp").astype(jnp.float32)
     mid = (stream.astype(jnp.float32) + summed).astype(jnp.bfloat16)
     mid_wide = mid.astype(jnp.float32)
     normed = (

time: 401 us -> 435 us (1.085)
  waiting for transfers between devices: 274 us -> 305 us
    psum x1 -> x0, waiting for transfers between devices: 36.5 us -> none  [shards(): lax.psum(partial_value.astype(jnp.bfloat16), 'tp').astype(jnp.float32)]
    all_gather x0 -> x1, waiting for transfers between devices: none -> 34.1 us  [gather_and_add(): terms = lax.all_gather(shard, name, axis=0, tiled=False)]
    all_gather x1, waiting for transfers between devices: 88 us -> 121 us  [shards(): lax.all_gather(up_weight, 'sp', axis=0, tiled=True)]
where the time goes in v1:
time: 435 us; the launch traced here: 434 us
  waiting for transfers between devices  305 us (70%)
  blocking collectives  64.3 us (15%)
  matrix products  28.8 us (7%)
  other arithmetic  18.3 us (4%)
  between operations  13.3 us (3%)
  local copies, waits for them, and re-layouts  4.36 us (1%)
    all_gather x1, waiting for transfers between devices, shards(): lax.all_gather(down_weight, 'sp', axis=1, tiled=True)  125 us
    all_gather x1, waiting for transfers between devices, shards(): lax.all_gather(up_weight, 'sp', axis=0, tiled=True)  121 us
    all_gather x1, waiting for transfers between devices, gather_and_add(): terms = lax.all_gather(shard, name, axis=0, tiled=False)  34.1 us
    all_gather x1, blocking collectives, shards(): key_rows = lax.all_gather(prepared_keys, 'sp', axis=0, tiled=True)  33 us
    all_gather x1, blocking collectives, shards(): value_rows = lax.all_gather(values, 'sp', axis=0, tiled=True)  31.3 us
    reduce_scatter x1, waiting for transfers between devices, shards(): lax.psum_scatter(down_part.astype(jnp.bfloat16), 'tp', scatter_dimension=...  23.1 us
    dot_general x1, matrix products, shards(): jnp.dot(hidden, lax.all_gather(down_weight, 'sp', axis=1, tiled=True), pr...  11.6 us
  transfers between devices with their start and end apart: 4, of which 4 were waited for; matrix products, arithmetic and copies ran while one was open for 1% of the time, Pallas kernels for 0%

profile of v1, /device:TPU:0, one launch (start us, length us, event | category | flops | bytes accessed | tf_op | source)
XLA Modules:
  0.0 434.2 jit_solution(17631543963495231398)
XLA Ops:
  6.5 0.0 copy-start
  6.5 0.0 all-gather.9.cloned.1.call-start
  6.6 1.2 copy.18
  7.8 0.3 reshape.165
  8.1 0.1 bitcast_reduce_fusion.1
  8.1 0.9 copy.17
  9.1 0.1 reshape.164
  9.2 0.8 mul.244
  10.0 0.1 broadcast_multiply_fusion.1
  10.1 0.1 fusion.28
  10.2 0.3 multiply_multiply_fusion
  10.5 0.7 subtract_convert_fusion
  11.1 0.6 pad_maximum_fusion
  11.7 0.1 convert_element_type.83
  11.9 0.8 mul.225
  12.6 0.1 multiply_multiply_fusion.1
  12.7 0.2 subtract_convert_fusion.1
  12.9 0.2 pad_maximum_fusion.1
  13.1 33.0 %all_gather.18 = bf16[2048,128]{0,1:T(8,128)(2,1)S(1)} all-gather(bf16[256,128]{0,1:T(8,128)(2,1)S(1)} %convert_element_type.81), channel_id=1, replica_groups=mesh['sp'=8,'tp'=4] {'sp'}, dimensions={0}, use_global_device_ids=true | all-gather | bytes 589824 | tf_op jit(solution)/shard_map/all_gather | solution.py:81
  46.2 8.1 %bitcast_reduce_fusion = (f32[2,4,256]{2,1,0:T(4,128)S(1)}, f32[2,2048,256,4]{2,1,3,0:T(8,128)}) fusion(bf16[2048,2,64,1]{0,2,3,1:T(8,128)(2,1)S(1)} %bitcast.65, bf16[256,2,4,64]{0,3,2,1:T(8,128)(2,1)S(1)} %convert_element_type.83), kind=kOutput, calls=%fused_computation.1 | convolution fusion | flops 545257472 | bytes 17571840 | tf_op jit(solution)/shard_map/while/body/eval_jaxpr/qhgd,khd->hgqk/dot_general | solution.py:46
  54.3 0.0 copy-start.1
  54.3 8.5 %fusion.1 = f32[2,4,256]{2,1,0:T(4,128)S(1)} fusion(f32[2,2048,256,4]{2,1,3,0:T(8,128)} %get-tuple-element.42, f32[2,4,256]{2,1,0:T(4,128)S(1)} %get-tuple-element.38), kind=kLoop, calls=%fused_computation.3 | loop fusion | flops 12580864 | bytes 16793600 | tf_op jit(solution)/shard_map/while/body/eval_jaxpr/reduce_sum | solution.py:51
  62.8 0.0 copy-done.1
  62.9 31.3 %all_gather.19 = bf16[2048,128]{1,0:T(8,128)(2,1)S(1)} all-gather(bf16[256,128]{1,0:T(8,128)(2,1)S(1)} %copy-done.1), channel_id=1, replica_groups=mesh['sp'=8,'tp'=4] {'sp'}, dimensions={0}, use_global_device_ids=true | all-gather | bytes 589824 | tf_op jit(solution)/shard_map/all_gather | solution.py:82
  94.1 0.2 copy.19
  94.4 7.4 %fusion.22 = bf16[256,2,4,64]{0,3,2,1:T(8,128)(2,1)S(1)} fusion(bf16[2048,2,64,1]{0,2,3,1:T(8,128)(2,1)S(1)} %bitcast.64, f32[2,2048,256,4]{2,1,3,0:T(8,128)} %get-tuple-element.42, f32[2,4,256]{2,1,0:T(4,128)S(1)} %get-tuple-element.38, f32[256,2,4]{0,2,1:T(4,128)S(1)} %bitcast_add_fusion, f32[256,2,4]{0,2,1:T(4,128)S(1)} %get-tuple-element.37), kind=kOutput, calls=%fused_computation.22 | convolution fusion | flops 549847040 | bytes 17588224 | tf_op jit(solution)/shard_map/while/body/eval_jaxpr/hgqk,khd->hgqd/dot_general | solution.py:52
  101.7 0.0 copy-start.2
  101.7 0.0 copy-done
  101.7 1.7 convolution_convert_fusion
  103.5 0.0 all-gather.9.cloned.1.call-update
  103.5 0.0 all-gather.5.cloned.1.call-start
  103.5 0.7 all-gather.5.cloned.1.call-update
  104.2 0.0 all-gather.7.cloned.1.call-start
  104.3 0.7 all-gather.7.cloned.1.call-update
  105.0 0.2 reduce-scatter.2.cloned.1.call-start
  105.2 34.1 %all-gather.9.cloned.1.call-done = bf16[1024,2048]{1,0:T(8,128)(2,1)} async-done(((bf16[256,2048]{1,0:T(8,128)(2,1)}), bf16[1024,2048]{1,0:T(8,128)(2,1)}) %all-gather.9.cloned.1.call-update) | async-done | bytes 4194320 | tf_op jit(solution)/shard_map/all_gather | solution.py:13
  139.3 3.1 reduce_sum.55
  142.4 2.6 fusion.7
  145.0 121.0 %all-gather.5.cloned.1.call-done = bf16[2048,2048]{1,0:T(8,128)(2,1)} async-done(((bf16[256,2048]{1,0:T(8,128)(2,1)}), bf16[2048,2048]{1,0:T(8,128)(2,1)}) %all-gather.5.cloned.1.call-update) | async-done | bytes 8388624 | tf_op jit(solution)/shard_map/all_gather | solution.py:110
  265.9 125.2 %all-gather.7.cloned.1.call-done = bf16[2048,2048]{1,0:T(8,128)(2,1)} async-done(((bf16[2048,256]{1,0:T(8,128)(2,1)}), bf16[2048,2048]{1,0:T(8,128)(2,1)}) %all-gather.7.cloned.1.call-update) | async-done | bytes 8388624 | tf_op jit(solution)/shard_map/all_gather | solution.py:116
  391.1 0.0 copy-done.2
  391.1 11.6 %convolution_convert_fusion.1 = bf16[256,2048]{1,0:T(8,128)(2,1)} fusion(bf16[2048,2048]{1,0:T(8,128)(2,1)} %all-gather.7.cloned.1.call-done, bf16[2048,2048]{1,0:T(8,128)(2,1)} %all-gather.5.cloned.1.call-done, bf16[256,2048]{1,0:T(8,128)(2,1)} %get-tuple-element.20, f32[2048]{0:T(1024)S(1)} %copy-done.2, f32[256]{0:T(256)S(1)} %add_rsqrt_fusion.2), kind=kOutput, calls=%fused_computation.12 | convolution fusion | flops 4299161600 | bytes 18883584 | tf_op jit(solution)/shard_map/dot_general | solution.py:114
  402.8 0.0 reduce-scatter.2.cloned.1.call-update
  402.8 23.1 %reduce-scatter.2.cloned.1.call-done = bf16[256,512]{1,0:T(8,128)(2,1)} async-done(((bf16[256,2048]{1,0:T(8,128)(2,1)}), bf16[256,512]{1,0:T(8,128)(2,1)}) %reduce-scatter.2.cloned.1.call-update) | async-done | bytes 262160 | tf_op jit(solution)/shard_map/reduce_scatter | solution.py:119
  425.9 1.8 add_convert_fusion.1
  (9 shorter events, 0.1 us)
Async XLA Ops:
  6.5 95.2 %copy-start = (bf16[512,2048]{1,0:T(8,128)(2,1)S(1)}, bf16[512,2048]{1,0:T(8,128)(2,1)}, u32[]{:S(2)}) copy-start(bf16[512,2048]{1,0:T(8,128)(2,1)} %param.16) | copy-start | bytes 6291460
  6.5 132.8 %all-gather.9.cloned.1.call-start = ((), (), s32[]{:S(2)}) async-start(), calls=%async_computation.4 | async-start | bytes 5242880 | tf_op jit(solution)/shard_map/all_gather | solution.py:13
  54.3 8.6 %copy-start.1 = (bf16[256,128]{1,0:T(8,128)(2,1)S(1)}, bf16[256,128]{1,0:T(8,128)(2,1)}, u32[]{:S(2)}) copy-start(bf16[256,128]{1,0:T(8,128)(2,1)} %param.12) | copy-start | bytes 196612
  101.7 289.4 %copy-start.2 = (f32[2048]{0:T(1024)S(1)}, f32[2048]{0:T(1024)}, u32[]{:S(2)}) copy-start(f32[2048]{0:T(1024)} %param.17) | copy-start | bytes 24580
  103.5 162.4 %all-gather.5.cloned.1.call-start = ((), (), s32[]{:S(2)}) async-start(), calls=%async_computation.1 | async-start | bytes 9437184 | tf_op jit(solution)/shard_map/all_gather | solution.py:110
  104.2 286.9 %all-gather.7.cloned.1.call-start = ((), (), s32[]{:S(2)}) async-start(), calls=%async_computation.2 | async-start | bytes 9437184 | tf_op jit(solution)/shard_map/all_gather | solution.py:116
  105.0 320.9 %reduce-scatter.2.cloned.1.call-start = ((), (), s32[]{:S(2)}) async-start(), calls=%async_computation.3 | async-start | bytes 1310720 | tf_op jit(solution)/shard_map/reduce_scatter | solution.py:119
Sparse Core Ops, SparseCore 0:
  103.6 35.6 all-gather.8
  141.4 124.4 all-gather.4
  268.0 123.1 all-gather.6
  402.9 22.9 reduce-scatter.1
